TPU v7x, 32 devices: a whole 2x2x4 slice. The times are simulated.
32 devices in a mesh: sp: 8 (over z, y), tp: 4 (over x, core).
Axes of the slice: x: 2, y: 2, z: 4, core: 2. Of those that a mesh axis runs over, the one named last changes fastest.
Arguments:
- inputs: bfloat16 [2, 1024, 2048], P(None, 'sp'), may hold values from -6 to 6
- norm_gain: float32 [2048], replicated, may hold values from 0.1 to 1.9
- query_weight: bfloat16 [2048, 1024], P('sp', 'tp'), may hold values from -0.125 to 0.125
- key_weight: bfloat16 [2048, 256], P('sp', 'tp'), may hold values from -0.125 to 0.125
- value_weight: bfloat16 [2048, 256], P('sp', 'tp'), may hold values from -0.125 to 0.125
- query_gain: float32 [64], replicated, may hold values from 0.1 to 24
- key_gain: float32 [64], replicated, may hold values from 0.1 to 1.9
- forget_cache: float32 [2, 16, 1024], P(None, 'tp'), may hold values from -104 to 0, as said below
- rec_in_weight: bfloat16 [2048, 1024], P('sp', 'tp'), may hold values from -0.125 to 0.125
- rec_gate_weight: bfloat16 [2048, 1024], P('sp', 'tp'), may hold values from -0.125 to 0.125
- conv_weight: bfloat16 [4, 1024], P(None, 'tp'), may hold values from -3 to 3
- decay_gate_weight: bfloat16 [16, 64, 64], P('tp'), may hold values from -0.75 to 0.75
- input_gate_weight: bfloat16 [16, 64, 64], P('tp'), may hold values from -0.75 to 0.75
- decay_param: float32 [1024], P('tp'), may hold values from 4 to 16
- decay_extra: float32 [2, 1024, 1024], P(None, 'sp', 'tp'), may hold values from -2 to 0
- attn_out_gain: float32 [1024], P('tp'), may hold values from 0.1 to 1.9
- rec_out_gain: float32 [1024], P('tp'), may hold values from 0.1 to 1.9
- out_att_weight: bfloat16 [1024, 2048], P('tp'), may hold values from -0.125 to 0.125
- out_rec_weight: bfloat16 [1024, 2048], P('tp'), may hold values from -0.125 to 0.125
Outputs:
- mixed: bfloat16 [2, 1024, 2048], P(None, 'sp', 'tp')
Inputs may be any that keep to these rules, and one draw needn't show every extreme that they name: `forget_cache`: Non-increasing along the positions of each sequence and head.
All inputs are finite; a program needn't handle non-finite values.
Results may differ from a plain program's by a relative error of at most 0.012.
The roundings to bfloat16 on the way count: a program that leaves them out, or rounds other values in their place, can miss the bound.
Values may be sent and summed in bfloat16 or wider, within the bound.
A program may use at most 128 MiB of HBM per device.

v0:
```python
import jax
import jax.numpy as jnp
from jax import lax
from jax.sharding import PartitionSpec as P

D = 2048
LRU_BLOCK = 64
CONV_TAPS = 4
lru_const = 8.0
norm_eps = 1e-06


def from_behind(value, axis, steps):
    count = lax.axis_size(axis)
    leading, last = (max(0, -steps), min(count, count - steps))
    return lax.ppermute(value, axis, [(source, source + steps) for source in range(leading, last)])


def rms_scale(values, gain):
    multiplier = lax.rsqrt(jnp.mean(values * values, axis=-1, keepdims=True) + norm_eps)
    return values * multiplier * gain


def merge_state(earlier, later):
    return (earlier[0] * later[0], later[0] * earlier[1] + later[1])


def block_length(length, span):
    shards = max(length // span, 1)
    group_size = 1
    for trial_size in range(1, shards + 1):
        if shards % trial_size == 0 and trial_size * span <= 1024:
            group_size = trial_size
    sub_size = group_size * span
    if length % sub_size:
        sub_size = length
    return sub_size


def body(
    inputs,
    norm_gain,
    query_weight,
    key_weight,
    value_weight,
    query_gain,
    key_gain,
    forget_cache,
    rec_in_weight,
    rec_gate_weight,
    conv_weight,
    decay_gate_weight,
    input_gate_weight,
    decay_param,
    decay_extra,
    attn_out_gain,
    rec_out_gain,
    out_att_weight,
    out_rec_weight,
):
    seq_count, seq_span, model_width = inputs.shape
    row_count = seq_count * seq_span
    head_dim = query_gain.shape[0]
    att_local = query_weight.shape[1] // head_dim
    kv_local = key_weight.shape[1] // head_dim
    head_group = att_local // kv_local
    channels = rec_in_weight.shape[1]
    normed = rms_scale(
        inputs.reshape(row_count, model_width).astype(jnp.float32), norm_gain
    ).astype(jnp.bfloat16)
    normed_cols = normed.T
    row_contract = (((0,), (0,)), ((), ()))
    kv_cols = key_weight.shape[1]
    pieces = (
        lax.all_gather(query_weight, "sp", axis=0, tiled=True),
        lax.all_gather(key_weight, "sp", axis=0, tiled=True),
        lax.all_gather(value_weight, "sp", axis=0, tiled=True),
        lax.all_gather(rec_in_weight, "sp", axis=0, tiled=True),
        lax.all_gather(rec_gate_weight, "sp", axis=0, tiled=True),
    )
    query_proj, key_proj, value_sum, rec_in_sum, gate_proj = tuple(
        (
            lax.dot_general(
                normed_cols, weight_part, row_contract, preferred_element_type=jnp.float32
            )
            for weight_part in pieces
        )
    )
    queries = rms_scale(query_proj.reshape(row_count, att_local, head_dim), query_gain).astype(
        jnp.bfloat16
    )
    queries = queries.reshape(seq_count, seq_span, kv_local, head_group, head_dim).transpose(
        0, 2, 3, 1, 4
    )
    queries = queries.reshape(seq_count, kv_local, head_group * seq_span, head_dim)
    key_heads = rms_scale(key_proj.reshape(row_count, kv_local, head_dim), key_gain).astype(
        jnp.bfloat16
    )
    key_heads = key_heads.reshape(seq_count, seq_span, kv_cols)
    value_heads = value_sum.astype(jnp.bfloat16).reshape(seq_count, seq_span, kv_cols)
    key_value = jnp.concatenate([key_heads, value_heads], axis=2)
    my_first = lax.axis_index("sp") * seq_span
    own_gates = lax.dynamic_slice_in_dim(forget_cache, my_first, seq_span, 2)
    own_gates = own_gates.reshape(seq_count, kv_local, head_group, seq_span, 1)
    query_pos = my_first + jnp.tile(jnp.arange(seq_span, dtype=jnp.int32), head_group)
    scaling = head_dim ** (-0.5)
    start_state = (
        jnp.full((seq_count, kv_local, head_group * seq_span), -jnp.inf, jnp.float32),
        jnp.zeros((seq_count, kv_local, head_group * seq_span), jnp.float32),
        jnp.zeros((seq_count, kv_local, head_group * seq_span, head_dim), jnp.float32),
    )
    shard_part = lax.all_gather(key_value, "sp", axis=1, tiled=True)
    offset = jnp.int32(0)
    length = shard_part.shape[1]
    sub_size = block_length(length, seq_span)

    def one_step(block_index, carried_state):
        key_first = offset + block_index * sub_size

        def work(carried):
            top_score, totals, accum = carried
            block_rows = lax.dynamic_slice_in_dim(shard_part, block_index * sub_size, sub_size, 1)
            key_block = block_rows[:, :, :kv_cols].reshape(seq_count, sub_size, kv_local, head_dim)
            value_block = block_rows[:, :, kv_cols:].reshape(
                seq_count, sub_size, kv_local, head_dim
            )
            key_gates = lax.dynamic_slice_in_dim(forget_cache, key_first, sub_size, 2)
            key_gates = key_gates.reshape(seq_count, kv_local, head_group, 1, sub_size)
            scores = (
                jnp.einsum(
                    "bhqd,bkhd->bhqk", queries, key_block, preferred_element_type=jnp.float32
                )
                * scaling
            )
            scores = (
                scores.reshape(seq_count, kv_local, head_group, seq_span, sub_size)
                + own_gates
                - key_gates
            )
            scores = scores.reshape(seq_count, kv_local, head_group * seq_span, sub_size)
            visible = (
                query_pos[:, None] >= (key_first + jnp.arange(sub_size, dtype=jnp.int32))[None, :]
            )
            scores = jnp.where(visible, scores, -jnp.inf)
            new_top = jnp.maximum(top_score, jnp.max(scores, axis=-1))
            safe_top = jnp.where(jnp.isfinite(new_top), new_top, 0.0)
            weights = jnp.exp(scores - safe_top[..., None])
            fading = jnp.exp(top_score - safe_top)
            totals = totals * fading + jnp.sum(weights, axis=-1)
            accum = accum * fading[..., None] + jnp.einsum(
                "bhqk,bkhd->bhqd",
                weights.astype(jnp.bfloat16),
                value_block,
                preferred_element_type=jnp.float32,
            )
            return (new_top, totals, accum)

        return lax.cond(
            key_first < my_first + seq_span, work, lambda carried: carried, carried_state
        )

    top_score, totals, accum = lax.fori_loop(0, length // sub_size, one_step, start_state)
    attended = (accum / totals[..., None]).reshape(
        seq_count, kv_local, head_group, seq_span, head_dim
    )
    attended = attended.transpose(0, 3, 1, 2, 4).reshape(row_count, att_local, head_dim)
    att_normed = rms_scale(attended, attn_out_gain.reshape(att_local, head_dim)).astype(
        jnp.bfloat16
    )
    att_normed = att_normed.reshape(row_count, att_local * head_dim)
    rec_in = rec_in_sum.astype(jnp.bfloat16).reshape(seq_count, seq_span, channels)
    before = from_behind(rec_in[:, seq_span - (CONV_TAPS - 1) :, :], "sp", 1)
    extended = jnp.concatenate([before, rec_in], axis=1)
    conv = jnp.zeros((seq_count, seq_span, channels), jnp.float32)
    for tap in range(CONV_TAPS):
        conv = conv + extended[:, tap : tap + seq_span].astype(jnp.float32) * conv_weight[
            tap
        ].astype(jnp.float32)
    conv = conv.astype(jnp.bfloat16)
    blocks_local = decay_gate_weight.shape[0]
    grouped = conv.reshape(seq_count, seq_span, blocks_local, LRU_BLOCK)
    gate_decay = jnp.einsum(
        "bsnd,nde->bsne", grouped, decay_gate_weight, preferred_element_type=jnp.float32
    ).reshape(seq_count, seq_span, channels)
    gate_input = jnp.einsum(
        "bsnd,nde->bsne", grouped, input_gate_weight, preferred_element_type=jnp.float32
    ).reshape(seq_count, seq_span, channels)
    log_decay = (
        -lru_const * jax.nn.sigmoid(gate_decay) * jax.nn.softplus(-decay_param) + decay_extra
    )
    drive = (
        jnp.sqrt(-jnp.expm1(2.0 * log_decay))
        * jax.nn.sigmoid(gate_input)
        * conv.astype(jnp.float32)
    )
    cum_decay, local_state = lax.associative_scan(merge_state, (jnp.exp(log_decay), drive), axis=1)
    every_decay, every_state = (
        lax.all_gather(cum_decay[:, seq_span - 1][None], "sp", axis=0, tiled=True),
        lax.all_gather(local_state[:, seq_span - 1][None], "sp", axis=0, tiled=True),
    )
    prefix_decay, prefix_state = lax.associative_scan(
        merge_state, (every_decay, every_state), axis=0
    )
    position = lax.axis_index("sp")
    earlier_state = lax.dynamic_index_in_dim(
        prefix_state, jnp.maximum(position - 1, 0), 0, keepdims=False
    )
    entering = jnp.where(position > 0, earlier_state, 0.0)
    state = local_state + cum_decay * entering[:, None, :]
    gated = state * jax.nn.gelu(gate_proj.reshape(seq_count, seq_span, channels))
    rec_normed = rms_scale(
        gated.reshape(row_count, blocks_local, LRU_BLOCK),
        rec_out_gain.reshape(blocks_local, LRU_BLOCK),
    ).astype(jnp.bfloat16)
    rec_normed = rec_normed.reshape(row_count, channels)
    out_cols = D // lax.axis_size("tp")
    pieces = row_count * lax.axis_size("tp") // row_count
    terms = jnp.dot(att_normed, out_att_weight, preferred_element_type=jnp.float32) + jnp.dot(
        rec_normed, out_rec_weight, preferred_element_type=jnp.float32
    )
    mixed_cols = lax.psum_scatter(
        terms.reshape(row_count, pieces, out_cols)
        .transpose(1, 0, 2)
        .reshape(pieces * row_count, out_cols)
        .astype(jnp.bfloat16),
        "tp",
        scatter_dimension=0,
        tiled=True,
    )
    return mixed_cols.reshape(seq_count, seq_span, out_cols)


def solution(mesh):
    return jax.shard_map(
        body,
        mesh=mesh,
        in_specs=(
            P(None, "sp", None),
            P(),
            P("sp", "tp"),
            P("sp", "tp"),
            P("sp", "tp"),
            P(),
            P(),
            P(None, "tp", None),
            P("sp", "tp"),
            P("sp", "tp"),
            P(None, "tp"),
            P("tp", None, None),
            P("tp", None, None),
            P("tp"),
            P(None, "sp", "tp"),
            P("tp"),
            P("tp"),
            P("tp", None),
            P("tp", None),
        ),
        out_specs=P(None, "sp", "tp"),
        check_vma=False,
    )
```

profile of v0, /device:TPU:0, one launch (start us, length us, event | category | flops | bytes accessed | tf_op | source)
XLA Modules:
  0.0 263.9 jit_solution(10849590766930557368)
XLA Ops:
  12.4 33.4 %all_gather.25 = bf16[2048,64]{0,1:T(8,128)(2,1)S(1)} all-gather(bf16[256,64]{0,1:T(8,128)(2,1)} %param.24), channel_id=1, replica_groups=mesh['sp'=8,'tp'=4] {'sp'}, dimensions={0}, use_global_device_ids=true | all-gather | bytes 294912 | tf_op jit(solution)/shard_map/all_gather | solution.py:76
  45.8 31.4 %all_gather.26 = bf16[2048,64]{0,1:T(8,128)(2,1)S(1)} all-gather(bf16[256,64]{0,1:T(8,128)(2,1)} %param.25), channel_id=1, replica_groups=mesh['sp'=8,'tp'=4] {'sp'}, dimensions={0}, use_global_device_ids=true | all-gather | bytes 294912 | tf_op jit(solution)/shard_map/all_gather | solution.py:77
  79.3 29.7 %all_gather.27 = bf16[2,1024,128]{1,2,0:T(8,128)(2,1)} all-gather(bf16[2,128,128]{1,2,0:T(8,128)(2,1)S(1)} %pad_maximum_fusion.3), channel_id=1, replica_groups=mesh['sp'=8,'tp'=4] {'sp'}, dimensions={1}, use_global_device_ids=true | all-gather | bytes 589824 | tf_op jit(solution)/shard_map/all_gather | solution.py:112
  110.3 2.4 copy.49
  112.6 1.7 multiply_reduce_fusion.1
  114.6 6.3 %conditional.1 = ((f32[2,1,512]{2,0,1:T(2,128)S(1)}, f32[2,1,512,64]{2,3,0,1:T(8,128)S(1)})) conditional(s32[]{:T(128)} %convert_element_type.124, (f32[2,1,512]{2,0,1:T(2,128)S(1)}, f32[2,1,512,64]{2,3,0,1:T(8,128)S(1)}) %tuple.30, (s32[]{:T(128)}, s32[4,128]{1,0:T(4,128)S(1)}, bf16[2,1,4,128,64]{3,2,4,0,1:T(4,128)(2,1)S(1)}, ...), branch_computations={%region_3.4_spmd, %region_4.7_spmd} | conditional | flops 281680384 | bytes 17967226 | solution.py:158
  115.9 2.4 fusion.3
  118.4 1.8 fusion.1
  121.5 1.7 convolution_convert_fusion
  123.3 3.3 %collective-permute-start = (bf16[2,3,256]{2,1,0:T(4,128)(2,1)S(1)}, bf16[2,3,256]{2,1,0:T(4,128)(2,1)S(1)}, u32[]{:S(2)}, u32[]{:S(2)}) collective-permute-start(bf16[2,3,256]{2,1,0:T(4,128)(2,1)S(1)} %slice.399), channel_id=1, source_target_pairs={{0,4},{4,8},{8,12},{12,16},{16,20},{20,24},{24,28},{1,5},{5,9},{9,... | collective-permute-start | bytes 9224 | tf_op jit(solution)/shard_map/ppermute | solution.py:16
  132.0 2.0 convert_multiply_fusion
  134.7 1.6 slice.363
  137.3 1.6 slice.316
  152.8 2.1 pad.116
  155.7 1.6 add.383
  157.3 1.7 fusion.45
  160.5 2.3 pad.118
  163.6 26.3 %all-gather = f32[16,1,256]{2,1,0:T(1,128)S(1)} all-gather(f32[2,1,256]{2,1,0:T(1,128)S(1)} %slice_add_fusion.4), channel_id=2, replica_groups=mesh['sp'=8,'tp'=4] {'sp'}, dimensions={0}, use_global_device_ids=true | all-gather | bytes 18432 | tf_op jit(solution)/shard_map/all_gather | solution.py:199
  190.4 1.6 pad_maximum_fusion.2
  197.7 26.1 %all-gather.1 = f32[16,1,256]{2,1,0:T(1,128)S(1)} all-gather(f32[2,1,256]{2,1,0:T(1,128)S(1)} %slice_add_fusion.3), channel_id=3, replica_groups=mesh['sp'=8,'tp'=4] {'sp'}, dimensions={0}, use_global_device_ids=true | all-gather | bytes 18432 | tf_op jit(solution)/shard_map/all_gather | solution.py:198
  224.9 3.0 %fusion.73 = (f32[2,128,256]{2,1,0:T(8,128)}, f32[2,128,256]{2,1,0:T(8,128)}) fusion(bf16[2,128,2048]{2,1,0:T(8,128)(2,1)} %multiply_convert_fusion, bf16[2048,256]{1,0:T(8,128)(2,1)} %all-gather.10.cloned.1.call-done, f32[2,256]{1,0:T(2,128)S(1)} %fusion.65, f32[2,128,256]{2,1,0:T(8,128)S(1)} %pad.131, f32[2,128,256]{2,1,0:T(8,128)} %pad.132, ...), kind=kOutput, calls=%fused_computation.170 | convolution fusion | flops 269352960 | bytes 3672064 | tf_op jit(solution)/shard_map/dot_general | solution.py:83
  227.9 1.8 copy.64
  232.1 1.7 fusion.12
  234.9 22.5 %reduce-scatter.2.cloned.1.call-done = bf16[256,512]{1,0:T(8,128)(2,1)} async-done(((bf16[1024,512]{1,0:T(8,128)(2,1)}), bf16[256,512]{1,0:T(8,128)(2,1)}) %reduce-scatter.2.cloned.1.call-update) | async-done | bytes 262160 | tf_op jit(solution)/shard_map/reduce_scatter | solution.py:221
  (216 shorter events, 46.3 us)
Async XLA Ops:
  6.5 120.2 %copy-start = (bf16[256,2048]{1,0:T(8,128)(2,1)S(1)}, bf16[256,2048]{1,0:T(8,128)(2,1)}, u32[]{:S(2)}) copy-start(bf16[256,2048]{1,0:T(8,128)(2,1)} %param.38) | copy-start | bytes 3145732
  6.5 70.7 %copy-start.1 = (bf16[2,128,2048]{2,1,0:T(8,128)(2,1)S(1)}, bf16[2,128,2048]{2,1,0:T(8,128)(2,1)}, u32[]{:S(2)}) copy-start(bf16[2,128,2048]{2,1,0:T(8,128)(2,1)} %param.21) | copy-start | bytes 3145732
  6.5 103.7 %all-gather.6.cloned.1.call-start = ((), (), s32[]{:S(2)}) async-start(), calls=%async_computation.1 | async-start | bytes 1179648 | tf_op jit(solution)/shard_map/all_gather | solution.py:75
  7.3 114.3 %all-gather.8.cloned.1.call-start = ((), (), s32[]{:S(2)}) async-start(), calls=%async_computation.2 | async-start | bytes 1179648 | tf_op jit(solution)/shard_map/all_gather | solution.py:78
  8.0 216.8 %all-gather.10.cloned.1.call-start = ((), (), s32[]{:S(2)}) async-start(), calls=%async_computation.3 | async-start | bytes 1179648 | tf_op jit(solution)/shard_map/all_gather | solution.py:79
  8.7 248.6 %reduce-scatter.2.cloned.1.call-start = ((), (), s32[]{:S(2)}) async-start(), calls=%async_computation.4 | async-start | bytes 1310720 | tf_op jit(solution)/shard_map/reduce_scatter | solution.py:221
  77.2 2.0 copy-start.15
  78.2 30.7 %copy-start.8 = (f32[2048]{0:T(1024)S(1)}, f32[2048]{0:T(1024)}, u32[]{:S(2)}) copy-start(f32[2048]{0:T(1024)} %param.22) | copy-start | bytes 24580
  110.2 2.4 copy-start.2
  112.6 1.7 copy-start.16
  115.9 2.5 copy-start.6
  118.3 1.8 copy-start.3
  121.0 5.6 %copy-start.13 = (f32[256]{0:T(256)S(1)}, f32[256]{0:T(256)}, u32[]{:S(2)}) copy-start(f32[256]{0:T(256)} %param.36) | copy-start | bytes 3076
  123.2 4.6 %copy-start.9 = (f32[1,256]{1,0:T(1,128)S(1)}, f32[1,256]{1,0:T(1,128)}, u32[]{:S(2)}) copy-start(f32[1,256]{1,0:T(1,128)} %get-tuple-element.199) | copy-start | bytes 3076
  123.2 4.6 %copy-start.10 = (f32[1,256]{1,0:T(1,128)S(1)}, f32[1,256]{1,0:T(1,128)}, u32[]{:S(2)}) copy-start(f32[1,256]{1,0:T(1,128)} %get-tuple-element.200) | copy-start | bytes 3076
  123.2 4.6 %copy-start.11 = (f32[1,256]{1,0:T(1,128)S(1)}, f32[1,256]{1,0:T(1,128)}, u32[]{:S(2)}) copy-start(f32[1,256]{1,0:T(1,128)} %get-tuple-element.201) | copy-start | bytes 3076
  123.2 4.6 %copy-start.12 = (f32[1,256]{1,0:T(1,128)S(1)}, f32[1,256]{1,0:T(1,128)}, u32[]{:S(2)}) copy-start(f32[1,256]{1,0:T(1,128)} %get-tuple-element.202) | copy-start | bytes 3076
  123.3 4.6 %collective-permute-start = (bf16[2,3,256]{2,1,0:T(4,128)(2,1)S(1)}, bf16[2,3,256]{2,1,0:T(4,128)(2,1)S(1)}, u32[]{:S(2)}, u32[]{:S(2)}) collective-permute-start(bf16[2,3,256]{2,1,0:T(4,128)(2,1)S(1)} %slice.399), channel_id=1, source_target_pairs={{0,4},{4,8},{8,12},{12,16},{16,20},{20,24},{24,28},{1,5},{5,9},{9,... | collective-permute-start | bytes 9224 | tf_op jit(solution)/shard_map/ppermute | solution.py:16
  126.6 2.2 copy-start.17
  128.1 0.7 copy-start.7
  144.1 7.1 %copy-start.4 = (f32[2,31,256]{2,1,0:T(8,128)S(1)}, f32[2,31,256]{2,1,0:T(8,128)}, u32[]{:S(2)}) copy-start(f32[2,31,256]{2,1,0:T(8,128)} %slice.361) | copy-start | bytes 190468
  144.2 7.1 %copy-start.5 = (f32[2,31,256]{2,1,0:T(8,128)S(1)}, f32[2,31,256]{2,1,0:T(8,128)}, u32[]{:S(2)}) copy-start(f32[2,31,256]{2,1,0:T(8,128)} %slice.320) | copy-start | bytes 190468
  224.8 7.1 %copy-start.14 = (f32[256]{0:T(256)S(1)}, f32[256]{0:T(256)}, u32[]{:S(2)}) copy-start(f32[256]{0:T(256)} %param.37) | copy-start | bytes 3076
Sparse Core Ops, SparseCore 0:
  9.5 44.2 all-gather.5
  55.9 41.5 all-gather.7
  99.6 38.9 all-gather.9
  235.0 22.3 reduce-scatter.1
where the time goes:
time: 265 us; the launch traced here: 264 us
  blocking collectives  147 us (55%)
  local copies, waits for them, and re-layouts  35.4 us (13%)
  waiting for transfers between devices  25.4 us (10%)
  other arithmetic  24.8 us (9%)
  matrix products  14.1 us (5%)
  between operations  13.9 us (5%)
  starting transfers between devices  3.38 us (1%)
    all_gather x1, blocking collectives, body(): lax.all_gather(key_weight, 'sp', axis=0, tiled=True)  33.4 us
    all_gather x1, blocking collectives, body(): lax.all_gather(value_weight, 'sp', axis=0, tiled=True)  31.4 us
    all_gather x1, blocking collectives, body(): shard_part = lax.all_gather(key_value, 'sp', axis=1, tiled=True)  29.7 us
    all_gather x1, blocking collectives, body(): lax.all_gather(local_state[:, seq_span - 1][None], 'sp', axis=0, tiled=True)  26.3 us
    all_gather x1, blocking collectives, body(): lax.all_gather(cum_decay[:, seq_span - 1][None], 'sp', axis=0, tiled=True)  26.1 us
    reduce_scatter x1, waiting for transfers between devices, body(): lax.psum_scatter(terms.reshape(row_count, pieces, out_cols).transpose(1,...  22.5 us
    slice x44, local copies, waits for them, and re-layouts, body(): lax.associative_scan(merge_state, (jnp.exp(log_decay), drive), axis=1)  11.2 us
    pad x24, local copies, waits for them, and re-layouts, body(): lax.associative_scan(merge_state, (jnp.exp(log_decay), drive), axis=1)  10.2 us
  transfers between devices with their start and end apart: 5, of which 2 were waited for; matrix products, arithmetic and copies ran while one was open for 24% of the time, Pallas kernels for 0%

commit v1 on v0

--- a/solution.py
+++ b/solution.py
@@ -8,6 +8,24 @@
 CONV_TAPS = 4
 lru_const = 8.0
 norm_eps = 1e-06
+
+
+def compute_the_panels(x_part, in_dim):
+    x_part = jnp.moveaxis(x_part, 0, in_dim)
+    z2 = x_part.shape
+    return x_part.reshape(*z2[:in_dim], z2[in_dim] * z2[in_dim + 1], *z2[in_dim + 2 :])
+
+
+def pack_columns(local_block, axis_id):
+    frame_out = local_block[None]
+    n_chips = lax.axis_size(axis_id)
+    for i in range(n_chips.bit_length() - 1):
+        known = 1 << i
+        odd = lax.ppermute(frame_out, axis_id, tuple(((no, no ^ known) for no in range(n_chips))))
+        met_up = jnp.stack([frame_out, odd])
+        f_next = lax.axis_index(axis_id) >> i & 1
+        frame_out = jnp.where(f_next == 0, met_up, met_up[::-1]).reshape(-1, *local_block.shape)
+    return frame_out
 
 
 def from_behind(value, axis, steps):
@@ -71,10 +89,14 @@
     normed_cols = normed.T
     row_contract = (((0,), (0,)), ((), ()))
     kv_cols = key_weight.shape[1]
+
+    def direct_the_arrays(q_in, vector, d0):
+        return compute_the_panels(pack_columns(q_in, vector), d0)
+
     pieces = (
         lax.all_gather(query_weight, "sp", axis=0, tiled=True),
         lax.all_gather(key_weight, "sp", axis=0, tiled=True),
-        lax.all_gather(value_weight, "sp", axis=0, tiled=True),
+        direct_the_arrays(value_weight, "sp", 0),
         lax.all_gather(rec_in_weight, "sp", axis=0, tiled=True),
         lax.all_gather(rec_gate_weight, "sp", axis=0, tiled=True),
     )

time: 265 us -> 210 us (0.79)
  blocking collectives: 147 us -> 115 us
  local copies, waits for them, and re-layouts: 35.4 us -> 15.5 us
  other arithmetic: 24.8 us -> 10.8 us
  waiting for transfers between devices: 25.4 us -> 35.2 us
    all_gather x1 -> x0, blocking collectives: 31.4 us -> none  [body(): lax.all_gather(value_weight, 'sp', axis=0, tiled=True)]
    ppermute x0 -> x3, waiting for transfers between devices: none -> 11.2 us  [pack_columns(): lax.ppermute(frame_out, axis_id, tuple(((no, no ^ known) for no in range(...]
    slice x44, local copies, waits for them, and re-layouts: 11.2 us -> 0.95 us  [body(): lax.associative_scan(merge_state, (jnp.exp(log_decay), drive), axis=1)]
    pad x24, local copies, waits for them, and re-layouts: 10.2 us -> 0.78 us  [body(): lax.associative_scan(merge_state, (jnp.exp(log_decay), drive), axis=1)]
    add x13, other arithmetic: 4.97 us -> 0.13 us  [body(): lax.associative_scan(merge_state, (jnp.exp(log_decay), drive), axis=1)]
    add x13, other arithmetic: 4.34 us -> 0.24 us  [merge_state(): return (earlier[0] * later[0], later[0] * earlier[1] + later[1])]
    ppermute x0 -> x3, starting transfers between devices: none -> 3.2 us  [pack_columns(): lax.ppermute(frame_out, axis_id, tuple(((no, no ^ known) for no in range(...]
    concatenate x11, other arithmetic: 3.16 us -> 0.12 us  [body(): lax.associative_scan(merge_state, (jnp.exp(log_decay), drive), axis=1)]
  transfers between devices with their start and end apart: 5 -> 8, of which waited for: 2 -> 3; matrix products, arithmetic and copies ran while one was open for 24% -> 13% of each run, Pallas kernels for 0% -> 0%
where the time goes in v1:
time: 210 us; the launch traced here: 209 us
  blocking collectives  115 us (55%)
  waiting for transfers between devices  35.2 us (17%)
  local copies, waits for them, and re-layouts  15.5 us (7%)
  between operations  14.3 us (7%)
  matrix products  12.8 us (6%)
  other arithmetic  10.8 us (5%)
  starting transfers between devices  5.71 us (3%)
    all_gather x1, blocking collectives, body(): lax.all_gather(key_weight, 'sp', axis=0, tiled=True)  32 us
    all_gather x1, blocking collectives, body(): shard_part = lax.all_gather(key_value, 'sp', axis=1, tiled=True)  30.3 us
    all_gather x1, blocking collectives, body(): lax.all_gather(local_state[:, seq_span - 1][None], 'sp', axis=0, tiled=True)  26.2 us
    all_gather x1, blocking collectives, body(): lax.all_gather(cum_decay[:, seq_span - 1][None], 'sp', axis=0, tiled=True)  26.1 us
    reduce_scatter x1, waiting for transfers between devices, body(): lax.psum_scatter(terms.reshape(row_count, pieces, out_cols).transpose(1,...  22.5 us
    ppermute x3, waiting for transfers between devices, pack_columns(): lax.ppermute(frame_out, axis_id, tuple(((no, no ^ known) for no in range(...  11.2 us
    dot_general x5, matrix products, body(): lax.dot_general(normed_cols, weight_part, row_contract, preferred_element...  5.54 us
  transfers between devices with their start and end apart: 8, of which 3 were waited for; matrix products, arithmetic and copies ran while one was open for 13% of the time, Pallas kernels for 0%

profile of v1, /device:TPU:0, one launch (start us, length us, event | category | flops | bytes accessed | tf_op | source)
XLA Modules:
  0.0 209.0 jit_solution(6152858000602536622)
XLA Ops:
  8.1 3.1 %collective-permute-start = (bf16[1,256,64]{1,2,0:T(8,128)(2,1)}, bf16[1,256,64]{1,2,0:T(8,128)(2,1)S(1)}, u32[]{:S(2)}, u32[]{:S(2)}) collective-permute-start(bf16[1,256,64]{1,2,0:T(8,128)(2,1)} %bitcast.200), channel_id=1, source_target_pairs={{0,4},{4,0},{8,12},{12,8},{16,20},{20,16},{24,28},{28,24},{1,5},{5... | collective-permute-start | bytes 98312 | tf_op jit(solution)/shard_map/ppermute | solution.py:24
  11.2 1.5 multiply_reduce_fusion
  12.7 32.0 %all_gather.22 = bf16[2048,64]{0,1:T(8,128)(2,1)S(1)} all-gather(bf16[256,64]{0,1:T(8,128)(2,1)} %param.24), channel_id=1, replica_groups=mesh['sp'=8,'tp'=4] {'sp'}, dimensions={0}, use_global_device_ids=true | all-gather | bytes 294912 | tf_op jit(solution)/shard_map/all_gather | solution.py:98
  44.7 1.0 fusion.14
  48.5 4.7 %collective-permute-done.1 = bf16[2,256,64]{1,2,0:T(8,128)(2,1)S(1)} collective-permute-done((bf16[2,256,64]{1,2,0:T(8,128)(2,1)S(1)}, bf16[2,256,64]{1,2,0:T(8,128)(2,1)S(1)}, u32[]{:S(2)}, u32[]{:S(2)}) %collective-permute-start.1) | collective-permute-done | bytes 65568 | tf_op jit(solution)/shard_map/ppermute | solution.py:24
  53.5 6.6 %collective-permute-done.2 = bf16[4,256,64]{1,0,2:T(4,128)(2,1)S(1)} collective-permute-done((bf16[4,256,64]{1,0,2:T(4,128)(2,1)S(1)}, bf16[4,256,64]{1,0,2:T(4,128)(2,1)S(1)}, u32[]{:S(2)}, u32[]{:S(2)}) %collective-permute-start.2) | collective-permute-done | bytes 131104 | tf_op jit(solution)/shard_map/ppermute | solution.py:24
  61.2 30.3 %all_gather.23 = bf16[2,1024,128]{1,2,0:T(8,128)(2,1)} all-gather(bf16[2,128,128]{1,2,0:T(8,128)(2,1)S(1)} %pad_maximum_fusion.6), channel_id=1, replica_groups=mesh['sp'=8,'tp'=4] {'sp'}, dimensions={1}, use_global_device_ids=true | all-gather | bytes 589824 | tf_op jit(solution)/shard_map/all_gather | solution.py:134
  91.5 1.5 copy.51
  94.5 7.3 %conditional.1 = ((f32[2,1,512]{2,0,1:T(2,128)S(1)}, f32[2,1,512,64]{2,3,0,1:T(8,128)S(1)})) conditional(s32[]{:T(128)} %convert_element_type.126, (f32[2,1,512]{2,0,1:T(2,128)S(1)}, f32[2,1,512,64]{2,3,0,1:T(8,128)S(1)}) %tuple.30, (s32[]{:T(128)}, s32[4,128]{1,0:T(4,128)S(1)}, bf16[2,1,4,128,64]{3,2,4,0,1:T(4,128)(2,1)}, ...), branch_computations={%region_3.4_spmd, %region_4.0_spmd} | conditional | flops 281680384 | bytes 17967226 | solution.py:180
  96.8 2.4 %fusion.3 = (f32[2,512]{1,0:T(2,128)S(1)}, f32[2,512,1024]{2,1,0:T(8,128)S(1)}) fusion(f32[2,4,1024]{2,1,0:T(4,128)} %get-tuple-element.151, f32[2,512]{1,0:T(2,128)S(1)} %bitcast.193, pred[512,1024]{1,0:T(8,128)(4,1)S(1)} %iota_compare_fusion, bf16[2,512,64]{1,2,0:T(8,128)(2,1)S(1)} %reshape.368, bf16[2,1024,128]{1,2,0:T(8,128)(2,1)} %get-tuple-element.143), kind=kOutput, calls=%fused_computation.5 | convolution fusion | flops 139459584 | bytes 5152768 | tf_op jit(solution)/shard_map/while/body/eval_jaxpr/cond/branch_1_fun/bhqd,bkhd->bhqk/dot_general | solution.py:152
  99.2 1.8 fusion.1
  102.6 1.0 reshape.385
  104.7 1.7 convolution_convert_fusion
  106.5 2.4 %collective-permute-start.3 = (bf16[2,3,256]{2,1,0:T(4,128)(2,1)S(1)}, bf16[2,3,256]{2,1,0:T(4,128)(2,1)S(1)}, u32[]{:S(2)}, u32[]{:S(2)}) collective-permute-start(bf16[2,3,256]{2,1,0:T(4,128)(2,1)S(1)} %slice.399), channel_id=1, source_target_pairs={{0,4},{4,8},{8,12},{12,16},{16,20},{20,24},{24,28},{1,5},{5,9},{9,... | collective-permute-start | bytes 9224 | tf_op jit(solution)/shard_map/ppermute | solution.py:34
  109.1 1.8 fusion.76
  115.0 26.2 %all-gather = f32[16,1,256]{2,1,0:T(1,128)S(1)} all-gather(f32[2,1,256]{2,1,0:T(1,128)S(1)} %slice_add_fusion.4), channel_id=2, replica_groups=mesh['sp'=8,'tp'=4] {'sp'}, dimensions={0}, use_global_device_ids=true | all-gather | bytes 18432 | tf_op jit(solution)/shard_map/all_gather | solution.py:221
  141.5 26.1 %all-gather.1 = f32[16,1,256]{2,1,0:T(1,128)S(1)} all-gather(f32[2,1,256]{2,1,0:T(1,128)S(1)} %slice_add_fusion.3), channel_id=3, replica_groups=mesh['sp'=8,'tp'=4] {'sp'}, dimensions={0}, use_global_device_ids=true | all-gather | bytes 18432 | tf_op jit(solution)/shard_map/all_gather | solution.py:220
  168.1 2.4 %fusion.75 = (f32[2,128,256]{2,1,0:T(8,128)}, f32[2,128,256]{2,1,0:T(8,128)S(1)}) fusion(bf16[2,128,2048]{2,1,0:T(8,128)(2,1)S(1)} %multiply_convert_fusion, bf16[2048,256]{1,0:T(8,128)(2,1)} %all-gather.10.cloned.1.call-done, f32[2,256]{1,0:T(2,128)S(1)} %fusion.67, f32[2,128,256]{2,1,0:T(8,128)S(1)} %pad.131, f32[2,128,256]{2,1,0:T(8,128)S(1)} %pad.132, ...), kind=kOutput, calls=%fused_computation.178 | convolution fusion | flops 269352960 | bytes 3672064 | tf_op jit(solution)/shard_map/dot_general | solution.py:105
  170.5 1.9 copy.68
  172.4 1.9 mul.433
  176.1 1.0 fusion.41
  177.2 1.7 fusion.12
  178.9 1.1 copy.98
  180.0 22.5 %reduce-scatter.2.cloned.1.call-done = bf16[256,512]{1,0:T(8,128)(2,1)} async-done(((bf16[1024,512]{1,0:T(8,128)(2,1)}), bf16[256,512]{1,0:T(8,128)(2,1)}) %reduce-scatter.2.cloned.1.call-update) | async-done | bytes 262160 | tf_op jit(solution)/shard_map/reduce_scatter | solution.py:243
  (241 shorter events, 18.0 us)
Async XLA Ops:
  6.5 102.6 %copy-start = (bf16[256,2048]{1,0:T(8,128)(2,1)S(1)}, bf16[256,2048]{1,0:T(8,128)(2,1)}, u32[]{:S(2)}) copy-start(bf16[256,2048]{1,0:T(8,128)(2,1)} %param.38) | copy-start | bytes 3145732
  6.5 38.2 %copy-start.1 = (bf16[2,128,2048]{2,1,0:T(8,128)(2,1)S(1)}, bf16[2,128,2048]{2,1,0:T(8,128)(2,1)}, u32[]{:S(2)}) copy-start(bf16[2,128,2048]{2,1,0:T(8,128)(2,1)} %param.21) | copy-start | bytes 3145732
  6.5 39.2 %copy-start.9 = (f32[2048]{0:T(1024)S(1)}, f32[2048]{0:T(1024)}, u32[]{:S(2)}) copy-start(f32[2048]{0:T(1024)} %param.22) | copy-start | bytes 24580
  6.5 85.0 %all-gather.6.cloned.1.call-start = ((), (), s32[]{:S(2)}) async-start(), calls=%async_computation.1 | async-start | bytes 1179648 | tf_op jit(solution)/shard_map/all_gather | solution.py:97
  7.3 97.5 %all-gather.8.cloned.1.call-start = ((), (), s32[]{:S(2)}) async-start(), calls=%async_computation.2 | async-start | bytes 1179648 | tf_op jit(solution)/shard_map/all_gather | solution.py:100
  8.0 160.0 %all-gather.10.cloned.1.call-start = ((), (), s32[]{:S(2)}) async-start(), calls=%async_computation.3 | async-start | bytes 1179648 | tf_op jit(solution)/shard_map/all_gather | solution.py:101
  8.1 39.7 %collective-permute-start = (bf16[1,256,64]{1,2,0:T(8,128)(2,1)}, bf16[1,256,64]{1,2,0:T(8,128)(2,1)S(1)}, u32[]{:S(2)}, u32[]{:S(2)}) collective-permute-start(bf16[1,256,64]{1,2,0:T(8,128)(2,1)} %bitcast.200), channel_id=1, source_target_pairs={{0,4},{4,0},{8,12},{12,8},{16,20},{20,16},{24,28},{28,24},{1,5},{5... | collective-permute-start | bytes 98312 | tf_op jit(solution)/shard_map/ppermute | solution.py:24
  11.1 191.3 %reduce-scatter.2.cloned.1.call-start = ((), (), s32[]{:S(2)}) async-start(), calls=%async_computation.4 | async-start | bytes 1310720 | tf_op jit(solution)/shard_map/reduce_scatter | solution.py:243
  45.7 2.1 %copy-start.19 = (f32[256]{0:T(256)S(1)}, f32[256]{0:T(256)}, u32[]{:S(2)}) copy-start(f32[256]{0:T(256)} %param.34) | copy-start | bytes 3076
  47.8 5.4 %collective-permute-start.1 = (bf16[2,256,64]{1,2,0:T(8,128)(2,1)S(1)}, bf16[2,256,64]{1,2,0:T(8,128)(2,1)S(1)}, u32[]{:S(2)}, u32[]{:S(2)}) collective-permute-start(bf16[2,256,64]{1,2,0:T(8,128)(2,1)S(1)} %get-tuple-element.169), channel_id=1, source_target_pairs={{0,8},{4,12},{8,0},{12,4},{16,24},{20,28},{24,16},{28,20},{1,9},{5... | collective-permute-start | bytes 196616 | tf_op jit(solution)/shard_map/ppermute | solution.py:24
  48.5 12.6 %copy-start.20 = (f32[64]{0:T(128)S(1)}, f32[64]{0:T(128)}, u32[]{:S(2)}) copy-start(f32[64]{0:T(128)} %param.27) | copy-start | bytes 772
  53.3 6.8 %collective-permute-start.2 = (bf16[4,256,64]{1,0,2:T(4,128)(2,1)S(1)}, bf16[4,256,64]{1,0,2:T(4,128)(2,1)S(1)}, u32[]{:S(2)}, u32[]{:S(2)}) collective-permute-start(bf16[4,256,64]{1,0,2:T(4,128)(2,1)S(1)} %copy.53), channel_id=1, source_target_pairs={{0,16},{4,20},{8,24},{12,28},{16,0},{20,4},{24,8},{28,12},{1,17},{... | collective-permute-start | bytes 393224 | tf_op jit(solution)/shard_map/ppermute | solution.py:24
  94.5 10.2 %copy-start.3 = (bf16[256,2048]{1,0:T(8,128)(2,1)S(1)}, bf16[256,2048]{1,0:T(8,128)(2,1)}, u32[]{:S(2)}) copy-start(bf16[256,2048]{1,0:T(8,128)(2,1)} %copy-done.2) | copy-start | bytes 3145732
  96.7 2.5 %copy-start.8 = (f32[2,4,1024]{2,1,0:T(4,128)S(1)}, f32[2,4,1024]{2,1,0:T(4,128)}, u32[]{:S(2)}) copy-start(f32[2,4,1024]{2,1,0:T(4,128)} %get-tuple-element.151) | copy-start | bytes 98308 | tf_op jit(solution)/shard_map/while/body/eval_jaxpr/cond
  101.9 7.1 %copy-start.17 = (f32[256]{0:T(256)S(1)}, f32[256]{0:T(256)}, u32[]{:S(2)}) copy-start(f32[256]{0:T(256)} %param.36) | copy-start | bytes 3076
  104.7 4.2 %copy-start.6 = (f32[2,1,4,128,64]{3,0,4,2,1:T(2,128)S(1)}, f32[2,1,4,128,64]{3,0,4,2,1:T(2,128)}, u32[]{:S(2)}) copy-start(f32[2,1,4,128,64]{3,0,4,2,1:T(2,128)} %copy.57) | copy-start | bytes 786436
  106.5 4.5 %copy-start.13 = (f32[1,256]{1,0:T(1,128)S(1)}, f32[1,256]{1,0:T(1,128)}, u32[]{:S(2)}) copy-start(f32[1,256]{1,0:T(1,128)} %get-tuple-element.201) | copy-start | bytes 3076
  106.5 4.4 %copy-start.14 = (f32[1,256]{1,0:T(1,128)S(1)}, f32[1,256]{1,0:T(1,128)}, u32[]{:S(2)}) copy-start(f32[1,256]{1,0:T(1,128)} %get-tuple-element.202) | copy-start | bytes 3076
  106.5 4.4 %copy-start.15 = (f32[1,256]{1,0:T(1,128)S(1)}, f32[1,256]{1,0:T(1,128)}, u32[]{:S(2)}) copy-start(f32[1,256]{1,0:T(1,128)} %get-tuple-element.203) | copy-start | bytes 3076
  106.5 4.4 %copy-start.16 = (f32[1,256]{1,0:T(1,128)S(1)}, f32[1,256]{1,0:T(1,128)}, u32[]{:S(2)}) copy-start(f32[1,256]{1,0:T(1,128)} %get-tuple-element.204) | copy-start | bytes 3076
  106.5 4.4 %collective-permute-start.3 = (bf16[2,3,256]{2,1,0:T(4,128)(2,1)S(1)}, bf16[2,3,256]{2,1,0:T(4,128)(2,1)S(1)}, u32[]{:S(2)}, u32[]{:S(2)}) collective-permute-start(bf16[2,3,256]{2,1,0:T(4,128)(2,1)S(1)} %slice.399), channel_id=1, source_target_pairs={{0,4},{4,8},{8,12},{12,16},{16,20},{20,24},{24,28},{1,5},{5,9},{9,... | collective-permute-start | bytes 9224 | tf_op jit(solution)/shard_map/ppermute | solution.py:34
  109.0 2.3 %copy-start.22 = (bf16[4,64,64]{2,1,0:T(8,128)(2,1)S(1)}, bf16[4,64,64]{2,1,0:T(8,128)(2,1)}, u32[]{:S(2)}) copy-start(bf16[4,64,64]{2,1,0:T(8,128)(2,1)} %param.33) | copy-start | bytes 98308
  168.0 8.1 %copy-start.18 = (f32[256]{0:T(256)S(1)}, f32[256]{0:T(256)}, u32[]{:S(2)}) copy-start(f32[256]{0:T(256)} %param.37) | copy-start | bytes 3076
  170.5 6.7 %copy-start.4 = (f32[256,2048]{1,0:T(8,128)S(1)}, f32[256,2048]{1,0:T(8,128)}, u32[]{:S(2)}) copy-start(f32[256,2048]{1,0:T(8,128)} %fusion.76) | copy-start | bytes 6291460
  (8 other events, 9.7 us)
Sparse Core Ops, SparseCore 0:
  9.5 44.6 all-gather.5
  56.3 41.4 all-gather.7
  99.9 38.7 all-gather.9
  180.1 22.3 reduce-scatter.1
